TPU v7x, 32 devices: a whole 2x2x4 slice. The times are simulated.
32 devices in a mesh: sp: 16 (over z, y, x), tp: 2 (over core).
Axes of the slice: x: 2, y: 2, z: 4, core: 2. Of those that a mesh axis runs over, the one named last changes fastest.
Arguments:
- stream_in: bfloat16 [4096, 2048], P('sp'), may hold values from -6 to 6
- norm_gain: float32 [2, 2048], replicated, may hold values from 0.1 to 1.9
- value_weight: bfloat16 [2, 2048, 2048], P(None, 'sp', 'tp'), may hold values from -0.125 to 0.125
- gate_weight: bfloat16 [2, 2048, 2048], P(None, 'sp', 'tp'), may hold values from -0.125 to 0.125
- conv_taps: float32 [2, 31, 2048], P(None, None, 'tp'), may hold values from -5 to 5
- channel_gain: float32 [2, 2048], P(None, 'tp'), may hold values from 0.1 to 1.9
- out_weight: bfloat16 [2, 2048, 2048], P(None, 'tp', 'sp'), may hold values from -0.125 to 0.125
Outputs:
- stream_out: bfloat16 [4096, 2048], P('sp')
All inputs are finite; a program needn't handle non-finite values.
Results may differ from a plain program's by a relative error of at most 0.015.
Values may be sent and summed in bfloat16 or wider, within the bound.
A program may use at most 64 MiB of HBM per device.

v0:
```python
import jax
import jax.numpy as jnp
from jax import lax
from jax.sharding import PartitionSpec as P

LAYERS = 2
epsilon = 1e-05


def passed_along(value, axis, steps):
    count = lax.axis_size(axis)
    leading, last = (max(0, -steps), min(count, count - steps))
    return lax.ppermute(value, axis, [(source, source + steps) for source in range(leading, last)])


def body(stream_in, norm_gain, value_weight, gate_weight, conv_taps, channel_gain, out_weight):
    stream = stream_in
    tok_rows = stream_in.shape[0]
    width = stream_in.shape[1]
    kernel = conv_taps.shape[1]
    local_cols = value_weight.shape[2]
    for layer in range(LAYERS):
        wide = stream.astype(jnp.float32)
        normed = (
            wide
            * lax.rsqrt(jnp.mean(wide * wide, axis=1, keepdims=True) + epsilon)
            * norm_gain[layer]
        ).astype(jnp.bfloat16)
        value = jnp.dot(
            normed,
            lax.all_gather(value_weight[layer], "sp", axis=0, tiled=True),
            preferred_element_type=jnp.float32,
        )
        gate = jnp.dot(
            normed,
            lax.all_gather(gate_weight[layer], "sp", axis=0, tiled=True),
            preferred_element_type=jnp.float32,
        )
        gated = (value * jax.nn.sigmoid(gate)).astype(jnp.bfloat16)
        earlier = passed_along(gated[tok_rows - (kernel - 1) :], "sp", 1)
        padded = jnp.concatenate([earlier, gated], axis=0).astype(jnp.float32)
        taps = conv_taps[layer]
        filtered = jnp.zeros((tok_rows, local_cols), jnp.float32)
        for tap in range(kernel):
            filtered = filtered + taps[tap] * padded[tap : tap + tok_rows]
        sum_first, sum_second = lax.psum(
            (jnp.sum(filtered, axis=1), jnp.sum(filtered * filtered, axis=1)), "tp"
        )
        mean_value = (sum_first / width)[:, None]
        variance = (sum_second / width)[:, None] - mean_value * mean_value
        activated = jax.nn.silu(
            (filtered - mean_value) * lax.rsqrt(variance + epsilon) * channel_gain[layer]
        ).astype(jnp.bfloat16)
        whole_out = lax.all_gather(out_weight[layer], "sp", axis=1, tiled=True)
        terms = jnp.dot(activated, whole_out, preferred_element_type=jnp.float32)
        summed = lax.psum(terms.astype(jnp.bfloat16), "tp").astype(jnp.float32)
        stream = (wide + summed).astype(jnp.bfloat16)
    return stream


def solution(mesh):
    return jax.shard_map(
        body,
        mesh=mesh,
        in_specs=(
            P("sp", None),
            P(),
            P(None, "sp", "tp"),
            P(None, "sp", "tp"),
            P(None, None, "tp"),
            P(None, "tp"),
            P(None, "tp", "sp"),
        ),
        out_specs=P("sp", None),
        check_vma=False,
    )
```

profile of v0, /device:TPU:0, one launch (start us, length us, event | category | flops | bytes accessed | tf_op | source)
XLA Modules:
  0.0 556.1 jit_solution(6253315192449355150)
XLA Ops:
  6.5 2.0 fusion.142
  8.6 1.9 fusion.141
  12.0 76.4 %all-gather.15.cloned.1.call-done = bf16[1,2048,1024]{2,1,0:T(8,128)(2,1)} async-done(((bf16[1,128,1024]{2,1,0:T(8,128)(2,1)}), bf16[1,2048,1024]{2,1,0:T(8,128)(2,1)}) %all-gather.15.cloned.1.call-update) | async-done | bytes 4194320 | tf_op jit(solution)/shard_map/all_gather | solution.py:36
  88.5 3.6 fusion.56
  92.1 73.4 %all-gather.13.cloned.1.call-done = bf16[1,2048,1024]{2,1,0:T(8,128)(2,1)} async-done(((bf16[1,128,1024]{2,1,0:T(8,128)(2,1)}), bf16[1,2048,1024]{2,1,0:T(8,128)(2,1)}) %all-gather.13.cloned.1.call-update) | async-done | bytes 4194320 | tf_op jit(solution)/shard_map/all_gather | solution.py:31
  165.4 3.5 fusion.53
  169.0 3.4 collective-permute-start
  172.4 1.9 collective-permute-done
  174.4 5.8 %fusion.137 = (f32[256]{0:T(256)S(1)}, f32[256]{0:T(256)S(1)}, f32[256,1024]{1,0:T(8,128)S(1)}) fusion(f32[286,1024]{1,0:T(8,128)S(1)} %maximum_convert_fusion, f32[1024]{0:T(1024)S(1)} %bitcast.146, f32[1024]{0:T(1024)S(1)} %bitcast.147, f32[1024]{0:T(1024)S(1)} %bitcast.148, f32[1024]{0:T(1024)S(1)} %bitcast.149, f32[1024]{0:T(1024)S(1)} %bitcast.150, ...), kind=kLoop, calls=%fused_computation.185 | loop fusion | flops 16776704 | bytes 33683456 | tf_op jit(solution)/shard_map/reduce_sum | solution.py:47
  180.2 2.5 all-reduce.1
  182.7 72.8 %all-gather.17.cloned.1.call-done = bf16[1,1024,2048]{2,1,0:T(8,128)(2,1)} async-done(((bf16[1,1024,128]{2,1,0:T(8,128)(2,1)}), bf16[1,1024,2048]{2,1,0:T(8,128)(2,1)}) %all-gather.17.cloned.1.call-update) | async-done | bytes 4194320 | tf_op jit(solution)/shard_map/all_gather | solution.py:54
  255.5 4.7 fusion.12
  262.2 15.8 %all-reduce.5.cloned.1.call-done = bf16[256,2048]{1,0:T(8,128)(2,1)} async-done(((bf16[256,2048]{1,0:T(8,128)(2,1)}), bf16[256,2048]{1,0:T(8,128)(2,1)}) %all-reduce.5.cloned.1.call-update) | async-done | bytes 1048592 | tf_op jit(solution)/shard_map/psum | solution.py:56
  279.7 77.7 %all-gather.21.cloned.1.call-done = bf16[1,2048,1024]{2,1,0:T(8,128)(2,1)} async-done(((bf16[1,128,1024]{2,1,0:T(8,128)(2,1)}), bf16[1,2048,1024]{2,1,0:T(8,128)(2,1)}) %all-gather.21.cloned.1.call-update) | async-done | bytes 4194320 | tf_op jit(solution)/shard_map/all_gather | solution.py:36
  357.4 3.6 fusion.59
  361.0 73.3 %all-gather.19.cloned.1.call-done = bf16[1,2048,1024]{2,1,0:T(8,128)(2,1)} async-done(((bf16[1,128,1024]{2,1,0:T(8,128)(2,1)}), bf16[1,2048,1024]{2,1,0:T(8,128)(2,1)}) %all-gather.19.cloned.1.call-update) | async-done | bytes 4194320 | tf_op jit(solution)/shard_map/all_gather | solution.py:31
  434.3 3.5 fusion.50
  437.8 3.5 collective-permute-start.1
  443.2 5.8 %fusion.136 = (f32[256]{0:T(256)S(1)}, f32[256]{0:T(256)S(1)}, f32[256,1024]{1,0:T(8,128)S(1)}) fusion(f32[286,1024]{1,0:T(8,128)S(1)} %maximum_convert_fusion.1, f32[1024]{0:T(1024)S(1)} %bitcast.112, f32[1024]{0:T(1024)S(1)} %bitcast.113, f32[1024]{0:T(1024)S(1)} %bitcast.156, f32[1024]{0:T(1024)S(1)} %bitcast.157, f32[1024]{0:T(1024)S(1)} %bitcast.158, ...), kind=kLoop, calls=%fused_computation.184 | loop fusion | flops 16776704 | bytes 33683456 | tf_op jit(solution)/shard_map/reduce_sum | solution.py:47
  449.1 2.5 all-reduce
  451.5 72.8 %all-gather.23.cloned.1.call-done = bf16[1,1024,2048]{2,1,0:T(8,128)(2,1)} async-done(((bf16[1,1024,128]{2,1,0:T(8,128)(2,1)}), bf16[1,1024,2048]{2,1,0:T(8,128)(2,1)}) %all-gather.23.cloned.1.call-update) | async-done | bytes 4194320 | tf_op jit(solution)/shard_map/all_gather | solution.py:54
  524.3 4.7 fusion.15
  529.0 17.8 %all-reduce.7.cloned.1.call-done = bf16[256,2048]{1,0:T(8,128)(2,1)} async-done(((bf16[256,2048]{1,0:T(8,128)(2,1)}), bf16[256,2048]{1,0:T(8,128)(2,1)}) %all-reduce.7.cloned.1.call-update) | async-done | bytes 1048592 | tf_op jit(solution)/shard_map/psum | solution.py:56
  546.8 2.5 fusion.25
  (44 shorter events, 7.2 us)
Async XLA Ops:
  6.5 4.1 copy-start.1
  6.5 5.0 copy-start
  6.5 81.9 %all-gather.15.cloned.1.call-start = ((), (), s32[]{:S(2)}) async-start(), calls=%async_computation.3 | async-start | bytes 4456448 | tf_op jit(solution)/shard_map/all_gather | solution.py:36
  8.5 3.3 copy-start.2
  8.5 3.5 copy-start.3
  8.6 156.9 %all-gather.13.cloned.1.call-start = ((), (), s32[]{:S(2)}) async-start(), calls=%async_computation.2 | async-start | bytes 4456448 | tf_op jit(solution)/shard_map/all_gather | solution.py:31
  10.6 244.9 %all-gather.17.cloned.1.call-start = ((), (), s32[]{:S(2)}) async-start(), calls=%async_computation.4 | async-start | bytes 4456448 | tf_op jit(solution)/shard_map/all_gather | solution.py:54
  11.5 266.5 %all-reduce.5.cloned.1.call-start = ((), (), s32[]{:S(2)}) async-start(), calls=%async_computation | async-start | bytes 2097152 | tf_op jit(solution)/shard_map/psum | solution.py:56
  92.0 80.3 %copy-start.4 = (f32[2,1024]{1,0:T(2,128)S(1)}, f32[2,1024]{1,0:T(2,128)}, u32[]{:S(2)}) copy-start(f32[2,1024]{1,0:T(2,128)} %param.12) | copy-start | bytes 24580
  169.0 5.2 collective-permute-start
  260.2 97.2 %all-gather.21.cloned.1.call-start = ((), (), s32[]{:S(2)}) async-start(), calls=%async_computation.6 | async-start | bytes 4456448 | tf_op jit(solution)/shard_map/all_gather | solution.py:36
  260.8 173.5 %all-gather.19.cloned.1.call-start = ((), (), s32[]{:S(2)}) async-start(), calls=%async_computation.5 | async-start | bytes 4456448 | tf_op jit(solution)/shard_map/all_gather | solution.py:31
  261.4 262.9 %all-gather.23.cloned.1.call-start = ((), (), s32[]{:S(2)}) async-start(), calls=%async_computation.7 | async-start | bytes 4456448 | tf_op jit(solution)/shard_map/all_gather | solution.py:54
  262.1 284.6 %all-reduce.7.cloned.1.call-start = ((), (), s32[]{:S(2)}) async-start(), calls=%async_computation.1 | async-start | bytes 2097152 | tf_op jit(solution)/shard_map/psum | solution.py:56
  437.8 5.3 collective-permute-start.1
Sparse Core Ops, SparseCore 0:
  10.1 78.3 all-gather.14
  91.2 74.1 all-gather.12
  168.2 87.3 all-gather.16
  260.3 17.5 all-reduce.4
  280.6 76.7 all-gather.20
  360.0 74.1 all-gather.18
  437.0 87.3 all-gather.22
  529.1 17.5 all-reduce.6
where the time goes:
time: 557 us; the launch traced here: 556 us
  waiting for transfers between devices  485 us (87%)
  matrix products  23.6 us (4%)
  other arithmetic  16.5 us (3%)
  between operations  13.7 us (2%)
  starting transfers between devices  7.18 us (1%)
    all_gather x2, waiting for transfers between devices, body(): lax.all_gather(gate_weight[layer], 'sp', axis=0, tiled=True)  154 us
    all_gather x2, waiting for transfers between devices, body(): lax.all_gather(value_weight[layer], 'sp', axis=0, tiled=True)  147 us
    all_gather x2, waiting for transfers between devices, body(): whole_out = lax.all_gather(out_weight[layer], 'sp', axis=1, tiled=True)  146 us
    psum x2, waiting for transfers between devices, body(): summed = lax.psum(terms.astype(jnp.bfloat16), 'tp').astype(jnp.float32)  33.6 us
    reduce_sum x2, other arithmetic, body(): jnp.sum(filtered, axis=1)  11.6 us
  transfers between devices with their start and end apart: 10, of which 10 were waited for; matrix products, arithmetic and copies ran while one was open for 6% of the time, Pallas kernels for 0%

commit v1 on v0

--- a/solution.py
+++ b/solution.py
@@ -5,6 +5,16 @@
 
 LAYERS = 2
 epsilon = 1e-05
+
+
+def gather_by_hops(x, mesh_axis, d):
+    size = lax.axis_size(mesh_axis)
+    held, tiles = (x, [x])
+    for _ in range(size - 1):
+        held = lax.ppermute(held, mesh_axis, [(i, (i + 1) % size) for i in range(size)])
+        tiles.insert(0, held)
+    flat = jnp.concatenate(tiles, axis=d)
+    return jnp.roll(flat, (lax.axis_index(mesh_axis) + 1) * x.shape[d], axis=d)
 
 
 def passed_along(value, axis, steps):
@@ -51,7 +61,7 @@
         activated = jax.nn.silu(
             (filtered - mean_value) * lax.rsqrt(variance + epsilon) * channel_gain[layer]
         ).astype(jnp.bfloat16)
-        whole_out = lax.all_gather(out_weight[layer], "sp", axis=1, tiled=True)
+        whole_out = gather_by_hops(out_weight[layer], "sp", 1)
         terms = jnp.dot(activated, whole_out, preferred_element_type=jnp.float32)
         summed = lax.psum(terms.astype(jnp.bfloat16), "tp").astype(jnp.float32)
         stream = (wide + summed).astype(jnp.bfloat16)

time: 557 us -> 537 us (0.964)
  waiting for transfers between devices: 485 us -> 423 us
  local copies, waits for them, and re-layouts: 5.06 us -> 40.7 us
    ppermute x0 -> x30, waiting for transfers between devices: none -> 232 us  [gather_by_hops(): lax.ppermute(held, mesh_axis, [(i, (i + 1) % size) for i in range(size)])]
    all_gather x2 -> x0, waiting for transfers between devices: 146 us -> none  [body(): whole_out = lax.all_gather(out_weight[layer], 'sp', axis=1, tiled=True)]
    all_gather x2, waiting for transfers between devices: 154 us -> 77.7 us  [body(): lax.all_gather(gate_weight[layer], 'sp', axis=0, tiled=True)]
    all_gather x2, waiting for transfers between devices: 147 us -> 73.3 us  [body(): lax.all_gather(value_weight[layer], 'sp', axis=0, tiled=True)]
    unnamed x10 -> x112, local copies, waits for them, and re-layouts: 0.02 us -> 27.7 us
  transfers between devices with their start and end apart: 10 -> 38, of which waited for: 10 -> 35; matrix products, arithmetic and copies ran while one was open for 6% -> 8% of each run, Pallas kernels for 0% -> 0%
where the time goes in v1:
time: 537 us; the launch traced here: 536 us
  waiting for transfers between devices  423 us (79%)
  local copies, waits for them, and re-layouts  40.7 us (8%)
  matrix products  26.6 us (5%)
  other arithmetic  17.1 us (3%)
  between operations  14 us (3%)
  starting transfers between devices  9.48 us (2%)
    ppermute x30, waiting for transfers between devices, gather_by_hops(): lax.ppermute(held, mesh_axis, [(i, (i + 1) % size) for i in range(size)])  232 us
    all_gather x2, waiting for transfers between devices, body(): lax.all_gather(gate_weight[layer], 'sp', axis=0, tiled=True)  77.7 us
    all_gather x2, waiting for transfers between devices, body(): lax.all_gather(value_weight[layer], 'sp', axis=0, tiled=True)  73.3 us
    psum x2, waiting for transfers between devices, body(): summed = lax.psum(terms.astype(jnp.bfloat16), 'tp').astype(jnp.float32)  36.6 us
    unnamed x112, local copies, waits for them, and re-layouts  27.7 us
    reduce_sum x2, other arithmetic, body(): jnp.sum(filtered, axis=1)  11.6 us
    dot_general x2, matrix products, body(): terms = jnp.dot(activated, whole_out, preferred_element_type=jnp.float32)  11.2 us
  transfers between devices with their start and end apart: 38, of which 35 were waited for; matrix products, arithmetic and copies ran while one was open for 8% of the time, Pallas kernels for 0%

profile of v1, /device:TPU:0, one launch (start us, length us, event | category | flops | bytes accessed | tf_op | source)
XLA Modules:
  0.0 536.0 jit_solution(12080689881736592956)
XLA Ops:
  14.2 9.7 %collective-permute-done.17 = bf16[1024,128]{1,0:T(8,128)(2,1)S(1)} collective-permute-done((bf16[1024,128]{1,0:T(8,128)(2,1)S(1)}, bf16[1024,128]{1,0:T(8,128)(2,1)S(1)}, u32[]{:S(2)}, u32[]{:S(2)}) %collective-permute-start.17) | collective-permute-done | bytes 262176 | tf_op jit(solution)/shard_map/ppermute | solution.py:14
  23.8 6.5 %collective-permute-done.1 = bf16[1024,128]{1,0:T(8,128)(2,1)S(1)} collective-permute-done((bf16[1024,128]{1,0:T(8,128)(2,1)S(1)}, bf16[1024,128]{1,0:T(8,128)(2,1)S(1)}, u32[]{:S(2)}, u32[]{:S(2)}) %collective-permute-start.1) | collective-permute-done | bytes 262176 | tf_op jit(solution)/shard_map/ppermute | solution.py:14
  30.4 10.2 %collective-permute-done.18 = bf16[1024,128]{1,0:T(8,128)(2,1)S(1)} collective-permute-done((bf16[1024,128]{1,0:T(8,128)(2,1)S(1)}, bf16[1024,128]{1,0:T(8,128)(2,1)S(1)}, u32[]{:S(2)}, u32[]{:S(2)}) %collective-permute-start.18) | collective-permute-done | bytes 262176 | tf_op jit(solution)/shard_map/ppermute | solution.py:14
  63.2 6.3 %collective-permute-done.4 = bf16[1024,128]{1,0:T(8,128)(2,1)S(1)} collective-permute-done((bf16[1024,128]{1,0:T(8,128)(2,1)S(1)}, bf16[1024,128]{1,0:T(8,128)(2,1)S(1)}, u32[]{:S(2)}, u32[]{:S(2)}) %collective-permute-start.4) | collective-permute-done | bytes 262176 | tf_op jit(solution)/shard_map/ppermute | solution.py:14
  69.5 9.4 %collective-permute-done.21 = bf16[1024,128]{1,0:T(8,128)(2,1)S(1)} collective-permute-done((bf16[1024,128]{1,0:T(8,128)(2,1)S(1)}, bf16[1024,128]{1,0:T(8,128)(2,1)S(1)}, u32[]{:S(2)}, u32[]{:S(2)}) %collective-permute-start.21) | collective-permute-done | bytes 262176 | tf_op jit(solution)/shard_map/ppermute | solution.py:14
  78.9 10.2 %collective-permute-done.5 = bf16[1024,128]{1,0:T(8,128)(2,1)S(1)} collective-permute-done((bf16[1024,128]{1,0:T(8,128)(2,1)S(1)}, bf16[1024,128]{1,0:T(8,128)(2,1)S(1)}, u32[]{:S(2)}, u32[]{:S(2)}) %collective-permute-start.5) | collective-permute-done | bytes 262176 | tf_op jit(solution)/shard_map/ppermute | solution.py:14
  89.1 9.3 %collective-permute-done.22 = bf16[1024,128]{1,0:T(8,128)(2,1)S(1)} collective-permute-done((bf16[1024,128]{1,0:T(8,128)(2,1)S(1)}, bf16[1024,128]{1,0:T(8,128)(2,1)S(1)}, u32[]{:S(2)}, u32[]{:S(2)}) %collective-permute-start.22) | collective-permute-done | bytes 262176 | tf_op jit(solution)/shard_map/ppermute | solution.py:14
  104.7 11.5 %collective-permute-done.23 = bf16[1024,128]{1,0:T(8,128)(2,1)S(1)} collective-permute-done((bf16[1024,128]{1,0:T(8,128)(2,1)S(1)}, bf16[1024,128]{1,0:T(8,128)(2,1)S(1)}, u32[]{:S(2)}, u32[]{:S(2)}) %collective-permute-start.23) | collective-permute-done | bytes 262176 | tf_op jit(solution)/shard_map/ppermute | solution.py:14
  116.3 11.2 %collective-permute-done.7 = bf16[1024,128]{1,0:T(8,128)(2,1)S(1)} collective-permute-done((bf16[1024,128]{1,0:T(8,128)(2,1)S(1)}, bf16[1024,128]{1,0:T(8,128)(2,1)S(1)}, u32[]{:S(2)}, u32[]{:S(2)}) %collective-permute-start.7) | collective-permute-done | bytes 262176 | tf_op jit(solution)/shard_map/ppermute | solution.py:14
  128.2 9.7 %collective-permute-done.24 = bf16[1024,128]{1,0:T(8,128)(2,1)S(1)} collective-permute-done((bf16[1024,128]{1,0:T(8,128)(2,1)S(1)}, bf16[1024,128]{1,0:T(8,128)(2,1)S(1)}, u32[]{:S(2)}, u32[]{:S(2)}) %collective-permute-start.24) | collective-permute-done | bytes 262176 | tf_op jit(solution)/shard_map/ppermute | solution.py:14
  137.9 11.2 %collective-permute-done.8 = bf16[1024,128]{1,0:T(8,128)(2,1)S(1)} collective-permute-done((bf16[1024,128]{1,0:T(8,128)(2,1)S(1)}, bf16[1024,128]{1,0:T(8,128)(2,1)S(1)}, u32[]{:S(2)}, u32[]{:S(2)}) %collective-permute-start.8) | collective-permute-done | bytes 262176 | tf_op jit(solution)/shard_map/ppermute | solution.py:14
  155.9 6.6 %collective-permute-done.9 = bf16[1024,128]{1,0:T(8,128)(2,1)S(1)} collective-permute-done((bf16[1024,128]{1,0:T(8,128)(2,1)S(1)}, bf16[1024,128]{1,0:T(8,128)(2,1)S(1)}, u32[]{:S(2)}, u32[]{:S(2)}) %collective-permute-start.9) | collective-permute-done | bytes 262176 | tf_op jit(solution)/shard_map/ppermute | solution.py:14
  163.3 7.5 %collective-permute-done.26 = bf16[1024,128]{1,0:T(8,128)(2,1)S(1)} collective-permute-done((bf16[1024,128]{1,0:T(8,128)(2,1)S(1)}, bf16[1024,128]{1,0:T(8,128)(2,1)S(1)}, u32[]{:S(2)}, u32[]{:S(2)}) %collective-permute-start.26) | collective-permute-done | bytes 262176 | tf_op jit(solution)/shard_map/ppermute | solution.py:14
  170.7 9.2 %collective-permute-done.10 = bf16[1024,128]{1,0:T(8,128)(2,1)S(1)} collective-permute-done((bf16[1024,128]{1,0:T(8,128)(2,1)S(1)}, bf16[1024,128]{1,0:T(8,128)(2,1)S(1)}, u32[]{:S(2)}, u32[]{:S(2)}) %collective-permute-start.10) | collective-permute-done | bytes 262176 | tf_op jit(solution)/shard_map/ppermute | solution.py:14
  191.7 11.2 %collective-permute-done.28 = bf16[1024,128]{1,0:T(8,128)(2,1)S(1)} collective-permute-done((bf16[1024,128]{1,0:T(8,128)(2,1)S(1)}, bf16[1024,128]{1,0:T(8,128)(2,1)S(1)}, u32[]{:S(2)}, u32[]{:S(2)}) %collective-permute-start.28) | collective-permute-done | bytes 262176 | tf_op jit(solution)/shard_map/ppermute | solution.py:14
  205.0 7.4 %collective-permute-done.12 = bf16[1024,128]{1,0:T(8,128)(2,1)S(1)} collective-permute-done((bf16[1024,128]{1,0:T(8,128)(2,1)S(1)}, bf16[1024,128]{1,0:T(8,128)(2,1)S(1)}, u32[]{:S(2)}, u32[]{:S(2)}) %collective-permute-start.12) | collective-permute-done | bytes 262176 | tf_op jit(solution)/shard_map/ppermute | solution.py:14
  213.1 7.3 %collective-permute-done.29 = bf16[1024,128]{1,0:T(8,128)(2,1)S(1)} collective-permute-done((bf16[1024,128]{1,0:T(8,128)(2,1)S(1)}, bf16[1024,128]{1,0:T(8,128)(2,1)S(1)}, u32[]{:S(2)}, u32[]{:S(2)}) %collective-permute-start.29) | collective-permute-done | bytes 262176 | tf_op jit(solution)/shard_map/ppermute | solution.py:14
  225.5 13.4 %collective-permute-done.30 = bf16[1024,128]{1,0:T(8,128)(2,1)} collective-permute-done((bf16[1024,128]{1,0:T(8,128)(2,1)S(1)}, bf16[1024,128]{1,0:T(8,128)(2,1)}, u32[]{:S(2)}, u32[]{:S(2)}) %collective-permute-start.30) | collective-permute-done | bytes 262176 | tf_op jit(solution)/shard_map/ppermute | solution.py:14
  241.1 9.1 %collective-permute-done.14 = bf16[1024,128]{1,0:T(8,128)(2,1)} collective-permute-done((bf16[1024,128]{1,0:T(8,128)(2,1)}, bf16[1024,128]{1,0:T(8,128)(2,1)}, u32[]{:S(2)}, u32[]{:S(2)}) %collective-permute-start.14) | collective-permute-done | bytes 262176 | tf_op jit(solution)/shard_map/ppermute | solution.py:14
  250.2 10.5 %collective-permute-done.31 = bf16[1024,128]{1,0:T(8,128)(2,1)} collective-permute-done((bf16[1024,128]{1,0:T(8,128)(2,1)}, bf16[1024,128]{1,0:T(8,128)(2,1)}, u32[]{:S(2)}, u32[]{:S(2)}) %collective-permute-start.31) | collective-permute-done | bytes 262176 | tf_op jit(solution)/shard_map/ppermute | solution.py:14
  310.8 16.6 %all-reduce.5.cloned.1.call-done = bf16[256,2048]{1,0:T(8,128)(2,1)} async-done(((bf16[256,2048]{1,0:T(8,128)(2,1)}), bf16[256,2048]{1,0:T(8,128)(2,1)}) %all-reduce.5.cloned.1.call-update) | async-done | bytes 1048592 | tf_op jit(solution)/shard_map/psum | solution.py:66
  329.2 77.7 %all-gather.15.cloned.1.call-done = bf16[1,2048,1024]{2,1,0:T(8,128)(2,1)} async-done(((bf16[1,128,1024]{2,1,0:T(8,128)(2,1)}), bf16[1,2048,1024]{2,1,0:T(8,128)(2,1)}) %all-gather.15.cloned.1.call-update) | async-done | bytes 4194320 | tf_op jit(solution)/shard_map/all_gather | solution.py:46
  410.5 73.3 %all-gather.13.cloned.1.call-done = bf16[1,2048,1024]{2,1,0:T(8,128)(2,1)} async-done(((bf16[1,128,1024]{2,1,0:T(8,128)(2,1)}), bf16[1,2048,1024]{2,1,0:T(8,128)(2,1)}) %all-gather.13.cloned.1.call-update) | async-done | bytes 4194320 | tf_op jit(solution)/shard_map/all_gather | solution.py:41
  506.6 20.0 %all-reduce.7.cloned.1.call-done = bf16[256,2048]{1,0:T(8,128)(2,1)} async-done(((bf16[256,2048]{1,0:T(8,128)(2,1)}), bf16[256,2048]{1,0:T(8,128)(2,1)}) %all-reduce.7.cloned.1.call-update) | async-done | bytes 1048592 | tf_op jit(solution)/shard_map/psum | solution.py:66
  (201 shorter events, 147.1 us)
Async XLA Ops:
  6.5 277.1 %all-gather.11.cloned.1.call-start = ((), (), s32[]{:S(2)}) async-start(), calls=%async_computation.3 | async-start | bytes 4456448 | tf_op jit(solution)/shard_map/all_gather | solution.py:46
  8.5 279.7 %all-gather.9.cloned.1.call-start = ((), (), s32[]{:S(2)}) async-start(), calls=%async_computation.2 | async-start | bytes 4456448 | tf_op jit(solution)/shard_map/all_gather | solution.py:41
  12.7 17.7 %collective-permute-start.1 = (bf16[1024,128]{1,0:T(8,128)(2,1)S(1)}, bf16[1024,128]{1,0:T(8,128)(2,1)S(1)}, u32[]{:S(2)}, u32[]{:S(2)}) collective-permute-start(bf16[1024,128]{1,0:T(8,128)(2,1)S(1)} %get-tuple-element.25), channel_id=1, source_target_pairs={{0,2},{2,4},{4,6},{6,8},{8,10},{10,12},{12,14},{14,16},{16,18},{18... | collective-permute-start | bytes 786440 | tf_op jit(solution)/shard_map/ppermute | solution.py:14
  23.8 16.7 %collective-permute-start.18 = (bf16[1024,128]{1,0:T(8,128)(2,1)S(1)}, bf16[1024,128]{1,0:T(8,128)(2,1)S(1)}, u32[]{:S(2)}, u32[]{:S(2)}) collective-permute-start(bf16[1024,128]{1,0:T(8,128)(2,1)S(1)} %collective-permute-done.17), channel_id=1, source_target_pairs={{0,2},{2,4},{4,6},{6,8},{8,10},{10,12},{12,14},{14,16},{16,18},{18... | collective-permute-start | bytes 786440 | tf_op jit(solution)/shard_map/ppermute | solution.py:14
  53.0 274.4 %all-reduce.5.cloned.1.call-start = ((), (), s32[]{:S(2)}) async-start(), calls=%async_computation | async-start | bytes 2097152 | tf_op jit(solution)/shard_map/psum | solution.py:66
  63.2 15.7 %collective-permute-start.21 = (bf16[1024,128]{1,0:T(8,128)(2,1)S(1)}, bf16[1024,128]{1,0:T(8,128)(2,1)S(1)}, u32[]{:S(2)}, u32[]{:S(2)}) collective-permute-start(bf16[1024,128]{1,0:T(8,128)(2,1)S(1)} %collective-permute-done.20), channel_id=1, source_target_pairs={{0,2},{2,4},{4,6},{6,8},{8,10},{10,12},{12,14},{14,16},{16,18},{18... | collective-permute-start | bytes 786440 | tf_op jit(solution)/shard_map/ppermute | solution.py:14
  69.5 19.6 %collective-permute-start.5 = (bf16[1024,128]{1,0:T(8,128)(2,1)S(1)}, bf16[1024,128]{1,0:T(8,128)(2,1)S(1)}, u32[]{:S(2)}, u32[]{:S(2)}) collective-permute-start(bf16[1024,128]{1,0:T(8,128)(2,1)S(1)} %collective-permute-done.4), channel_id=1, source_target_pairs={{0,2},{2,4},{4,6},{6,8},{8,10},{10,12},{12,14},{14,16},{16,18},{18... | collective-permute-start | bytes 786440 | tf_op jit(solution)/shard_map/ppermute | solution.py:14
  78.9 19.5 %collective-permute-start.22 = (bf16[1024,128]{1,0:T(8,128)(2,1)S(1)}, bf16[1024,128]{1,0:T(8,128)(2,1)S(1)}, u32[]{:S(2)}, u32[]{:S(2)}) collective-permute-start(bf16[1024,128]{1,0:T(8,128)(2,1)S(1)} %collective-permute-done.21), channel_id=1, source_target_pairs={{0,2},{2,4},{4,6},{6,8},{8,10},{10,12},{12,14},{14,16},{16,18},{18... | collective-permute-start | bytes 786440 | tf_op jit(solution)/shard_map/ppermute | solution.py:14
  98.4 17.9 %collective-permute-start.23 = (bf16[1024,128]{1,0:T(8,128)(2,1)S(1)}, bf16[1024,128]{1,0:T(8,128)(2,1)S(1)}, u32[]{:S(2)}, u32[]{:S(2)}) collective-permute-start(bf16[1024,128]{1,0:T(8,128)(2,1)S(1)} %collective-permute-done.22), channel_id=1, source_target_pairs={{0,2},{2,4},{4,6},{6,8},{8,10},{10,12},{12,14},{14,16},{16,18},{18... | collective-permute-start | bytes 786440 | tf_op jit(solution)/shard_map/ppermute | solution.py:14
  104.7 22.8 %collective-permute-start.7 = (bf16[1024,128]{1,0:T(8,128)(2,1)S(1)}, bf16[1024,128]{1,0:T(8,128)(2,1)S(1)}, u32[]{:S(2)}, u32[]{:S(2)}) collective-permute-start(bf16[1024,128]{1,0:T(8,128)(2,1)S(1)} %collective-permute-done.6), channel_id=1, source_target_pairs={{0,2},{2,4},{4,6},{6,8},{8,10},{10,12},{12,14},{14,16},{16,18},{18... | collective-permute-start | bytes 786440 | tf_op jit(solution)/shard_map/ppermute | solution.py:14
  116.3 21.6 %collective-permute-start.24 = (bf16[1024,128]{1,0:T(8,128)(2,1)S(1)}, bf16[1024,128]{1,0:T(8,128)(2,1)S(1)}, u32[]{:S(2)}, u32[]{:S(2)}) collective-permute-start(bf16[1024,128]{1,0:T(8,128)(2,1)S(1)} %collective-permute-done.23), channel_id=1, source_target_pairs={{0,2},{2,4},{4,6},{6,8},{8,10},{10,12},{12,14},{14,16},{16,18},{18... | collective-permute-start | bytes 786440 | tf_op jit(solution)/shard_map/ppermute | solution.py:14
  128.2 20.9 %collective-permute-start.8 = (bf16[1024,128]{1,0:T(8,128)(2,1)S(1)}, bf16[1024,128]{1,0:T(8,128)(2,1)S(1)}, u32[]{:S(2)}, u32[]{:S(2)}) collective-permute-start(bf16[1024,128]{1,0:T(8,128)(2,1)S(1)} %collective-permute-done.7), channel_id=1, source_target_pairs={{0,2},{2,4},{4,6},{6,8},{8,10},{10,12},{12,14},{14,16},{16,18},{18... | collective-permute-start | bytes 786440 | tf_op jit(solution)/shard_map/ppermute | solution.py:14
  137.9 18.0 %collective-permute-start.25 = (bf16[1024,128]{1,0:T(8,128)(2,1)S(1)}, bf16[1024,128]{1,0:T(8,128)(2,1)S(1)}, u32[]{:S(2)}, u32[]{:S(2)}) collective-permute-start(bf16[1024,128]{1,0:T(8,128)(2,1)S(1)} %collective-permute-done.24), channel_id=1, source_target_pairs={{0,2},{2,4},{4,6},{6,8},{8,10},{10,12},{12,14},{14,16},{16,18},{18... | collective-permute-start | bytes 786440 | tf_op jit(solution)/shard_map/ppermute | solution.py:14
  162.6 17.3 %collective-permute-start.10 = (bf16[1024,128]{1,0:T(8,128)(2,1)S(1)}, bf16[1024,128]{1,0:T(8,128)(2,1)S(1)}, u32[]{:S(2)}, u32[]{:S(2)}) collective-permute-start(bf16[1024,128]{1,0:T(8,128)(2,1)S(1)} %collective-permute-done.9), channel_id=1, source_target_pairs={{0,2},{2,4},{4,6},{6,8},{8,10},{10,12},{12,14},{14,16},{16,18},{18... | collective-permute-start | bytes 786440 | tf_op jit(solution)/shard_map/ppermute | solution.py:14
  185.1 17.8 %collective-permute-start.28 = (bf16[1024,128]{1,0:T(8,128)(2,1)S(1)}, bf16[1024,128]{1,0:T(8,128)(2,1)S(1)}, u32[]{:S(2)}, u32[]{:S(2)}) collective-permute-start(bf16[1024,128]{1,0:T(8,128)(2,1)S(1)} %collective-permute-done.27), channel_id=1, source_target_pairs={{0,2},{2,4},{4,6},{6,8},{8,10},{10,12},{12,14},{14,16},{16,18},{18... | collective-permute-start | bytes 786440 | tf_op jit(solution)/shard_map/ppermute | solution.py:14
  191.7 20.7 %collective-permute-start.12 = (bf16[1024,128]{1,0:T(8,128)(2,1)S(1)}, bf16[1024,128]{1,0:T(8,128)(2,1)S(1)}, u32[]{:S(2)}, u32[]{:S(2)}) collective-permute-start(bf16[1024,128]{1,0:T(8,128)(2,1)S(1)} %collective-permute-done.11), channel_id=1, source_target_pairs={{0,2},{2,4},{4,6},{6,8},{8,10},{10,12},{12,14},{14,16},{16,18},{18... | collective-permute-start | bytes 786440 | tf_op jit(solution)/shard_map/ppermute | solution.py:14
  202.9 17.6 %collective-permute-start.29 = (bf16[1024,128]{1,0:T(8,128)(2,1)S(1)}, bf16[1024,128]{1,0:T(8,128)(2,1)S(1)}, u32[]{:S(2)}, u32[]{:S(2)}) collective-permute-start(bf16[1024,128]{1,0:T(8,128)(2,1)S(1)} %collective-permute-done.28), channel_id=1, source_target_pairs={{0,2},{2,4},{4,6},{6,8},{8,10},{10,12},{12,14},{14,16},{16,18},{18... | collective-permute-start | bytes 786440 | tf_op jit(solution)/shard_map/ppermute | solution.py:14
  220.4 18.5 %collective-permute-start.30 = (bf16[1024,128]{1,0:T(8,128)(2,1)S(1)}, bf16[1024,128]{1,0:T(8,128)(2,1)}, u32[]{:S(2)}, u32[]{:S(2)}) collective-permute-start(bf16[1024,128]{1,0:T(8,128)(2,1)S(1)} %collective-permute-done.29), channel_id=1, source_target_pairs={{0,2},{2,4},{4,6},{6,8},{8,10},{10,12},{12,14},{14,16},{16,18},{18... | collective-permute-start | bytes 786440 | tf_op jit(solution)/shard_map/ppermute | solution.py:14
  225.5 24.6 %collective-permute-start.14 = (bf16[1024,128]{1,0:T(8,128)(2,1)}, bf16[1024,128]{1,0:T(8,128)(2,1)}, u32[]{:S(2)}, u32[]{:S(2)}) collective-permute-start(bf16[1024,128]{1,0:T(8,128)(2,1)} %collective-permute-done.13), channel_id=1, source_target_pairs={{0,2},{2,4},{4,6},{6,8},{8,10},{10,12},{12,14},{14,16},{16,18},{18... | collective-permute-start | bytes 786440 | tf_op jit(solution)/shard_map/ppermute | solution.py:14
  238.9 21.7 %collective-permute-start.31 = (bf16[1024,128]{1,0:T(8,128)(2,1)}, bf16[1024,128]{1,0:T(8,128)(2,1)}, u32[]{:S(2)}, u32[]{:S(2)}) collective-permute-start(bf16[1024,128]{1,0:T(8,128)(2,1)} %collective-permute-done.30), channel_id=1, source_target_pairs={{0,2},{2,4},{4,6},{6,8},{8,10},{10,12},{12,14},{14,16},{16,18},{18... | collective-permute-start | bytes 786440 | tf_op jit(solution)/shard_map/ppermute | solution.py:14
  250.2 19.9 %collective-permute-start.15 = (bf16[1024,128]{1,0:T(8,128)(2,1)}, bf16[1024,128]{1,0:T(8,128)(2,1)S(1)}, u32[]{:S(2)}, u32[]{:S(2)}) collective-permute-start(bf16[1024,128]{1,0:T(8,128)(2,1)} %collective-permute-done.14), channel_id=1, source_target_pairs={{0,2},{2,4},{4,6},{6,8},{8,10},{10,12},{12,14},{14,16},{16,18},{18... | collective-permute-start | bytes 786440 | tf_op jit(solution)/shard_map/ppermute | solution.py:14
  309.6 97.3 %all-gather.15.cloned.1.call-start = ((), (), s32[]{:S(2)}) async-start(), calls=%async_computation.5 | async-start | bytes 4456448 | tf_op jit(solution)/shard_map/all_gather | solution.py:46
  310.2 173.5 %all-gather.13.cloned.1.call-start = ((), (), s32[]{:S(2)}) async-start(), calls=%async_computation.4 | async-start | bytes 4456448 | tf_op jit(solution)/shard_map/all_gather | solution.py:41
  310.8 215.8 %all-reduce.7.cloned.1.call-start = ((), (), s32[]{:S(2)}) async-start(), calls=%async_computation.1 | async-start | bytes 2097152 | tf_op jit(solution)/shard_map/psum | solution.py:66
  (55 other events, 1047.4 us)
Sparse Core Ops, SparseCore 0:
  10.1 133.0 all-gather.10
  145.9 116.9 all-gather.8
  309.7 17.6 all-reduce.4
  330.1 76.7 all-gather.14
  409.5 74.1 all-gather.12
  506.7 19.8 all-reduce.6
